TPU v7x, 32 devices: a whole 2x2x4 slice. The times are simulated.
32 devices in a mesh: sp: 16 (over z, y, x), tp: 2 (over core).
Axes of the slice: x: 2, y: 2, z: 4, core: 2. Of those that a mesh axis runs over, the one named last changes fastest.
Arguments:
- resid: bfloat16 [2048, 2048], P(('sp', 'tp')), may hold values from -3 to 3
- queries: bfloat16 [2048, 2048], P('sp', 'tp'), may hold values from -6 to 6
- keys: bfloat16 [2048, 2048], P('sp', 'tp'), may hold values from -6 to 6
- values: bfloat16 [2048, 2048], P('sp', 'tp'), may hold values from -8 to 8
- doc_ids: int32 [2048], P('sp'), may hold values from 0 to 3, never falling along the last dimension, each value on 1 to 896 neighbouring positions
- score_offset: float32 [32], P('tp'), may hold values from -10 to -3
- out_weight: bfloat16 [2048, 2048], P('tp'), may hold values from -0.1875 to 0.1875
- norm_gain: float32 [2048], replicated, may hold values from 0.1 to 1.9
- gate_weight: bfloat16 [2048, 6144], P('sp', 'tp'), may hold values from -0.125 to 0.125
- up_weight: bfloat16 [2048, 6144], P('sp', 'tp'), may hold values from -0.125 to 0.125
- down_weight: bfloat16 [6144, 2048], P('tp', 'sp'), may hold values from -0.078125 to 0.078125
Outputs:
- layer_out: bfloat16 [2048, 2048], P(('sp', 'tp'))
Inputs may be any that keep to these rules, and one draw needn't show every extreme that they name: `doc_ids`: document numbers never fall along the sequence; each document has 1 to 896 positions, and one has exactly 896.
All inputs are finite; a program needn't handle non-finite values.
Results may differ from a plain program's by a relative error of at most 0.017.
Values may be sent and summed in bfloat16 or wider, within the bound.
A program may use at most 128 MiB of HBM per device.

v0:
```python
import jax
import jax.numpy as jnp
from jax import lax
from jax.sharding import PartitionSpec as P


def from_behind(shard, axis, by):
    peers = lax.axis_size(axis)
    pairs = [(i, i + by) for i in range(peers) if 0 <= i + by < peers]
    return lax.ppermute(shard, axis, pairs)


def as_sent(shard):
    return jax.tree.map(lambda a: a.astype(jnp.bfloat16) if a.dtype == jnp.float32 else a, shard)


def joined(earlier, later):
    return (
        jnp.concatenate([earlier[0], later[0]], axis=0),
        jnp.concatenate([earlier[1], later[1]], axis=0),
        jnp.concatenate([earlier[2], later[2]], axis=0),
    )


def block_update(carry, block, start, context):
    queries_h, q_pos, q_docs, offsets, scale = context
    total, carried = carry
    k_block, v_block, d_block = block
    count = k_block.shape[0]
    heads = offsets.shape[0]
    head_dim = queries_h.shape[2]

    def compute():
        key_pos = start + jnp.arange(count, dtype=jnp.int32)
        live = (
            (key_pos[None, :] >= 0)
            & (key_pos[None, :] < q_pos[:, None])
            & (d_block[None, :] == q_docs[:, None])
        )
        k_heads = k_block.reshape(count, heads, head_dim)
        v_heads = v_block.reshape(count, heads, head_dim)
        scores = (
            jnp.einsum("thd,shd->hts", queries_h, k_heads, preferred_element_type=jnp.float32)
            * scale
            + offsets[:, None, None]
        )
        log_keep = jnp.where(live[None], jax.nn.log_sigmoid(-scores), 0.0)
        tail = lax.cumsum(log_keep, axis=2, reverse=True) - log_keep + carried[:, :, None]
        weight = jnp.where(live[None], jnp.exp(jax.nn.log_sigmoid(scores) + tail), 0.0).astype(
            jnp.bfloat16
        )
        added = jnp.einsum("hts,shd->thd", weight, v_heads, preferred_element_type=jnp.float32)
        return (total + added, carried + jnp.sum(log_keep, axis=2))

    reached = (start + count > 0) & (d_block[-1] >= q_docs[0])
    return lax.cond(reached, compute, lambda: carry)


def on_device(
    resid,
    queries,
    keys,
    values,
    doc_ids,
    score_offset,
    out_weight,
    norm_gain,
    gate_weight,
    up_weight,
    down_weight,
):
    rows = queries.shape[0]
    heads = score_offset.shape[0]
    head_dim = queries.shape[1] // heads
    base = lax.axis_index("sp") * rows
    q_pos = base + jnp.arange(rows, dtype=jnp.int32)
    context = (
        queries.reshape(rows, heads, head_dim),
        q_pos,
        doc_ids,
        score_offset,
        head_dim ** (-0.5),
    )
    own = (keys, values, doc_ids)
    carry = (jnp.zeros((rows, heads, head_dim), jnp.float32), jnp.zeros((heads, rows), jnp.float32))
    nearest = from_behind((keys, values, doc_ids), "sp", 1)
    paired = joined(nearest, own)
    carry = block_update(carry, paired, base - rows, context)
    middle = from_behind((paired[0], paired[1], as_sent(paired[2])), "sp", 2)
    carry = block_update(carry, middle, base - 3 * rows, context)
    fourfold = joined(middle, paired)
    farthest = from_behind((fourfold[0], fourfold[1], as_sent(fourfold[2])), "sp", 4)
    carry = block_update(
        carry, tuple((piece[2 * rows :] for piece in farthest)), base - 5 * rows, context
    )
    carry = block_update(
        carry, tuple((piece[: 2 * rows] for piece in farthest)), base - 7 * rows, context
    )
    attended = carry[0].reshape(rows, heads * head_dim).astype(jnp.bfloat16)
    mixed_attn = lax.psum_scatter(
        jnp.dot(attended, out_weight, preferred_element_type=jnp.float32).astype(jnp.bfloat16),
        "tp",
        scatter_dimension=0,
        tiled=True,
    ).astype(jnp.float32)
    stream = resid.astype(jnp.float32) + mixed_attn
    normed = (
        stream * lax.rsqrt(jnp.mean(stream * stream, axis=1, keepdims=True) + 1e-06) * norm_gain
    ).astype(jnp.bfloat16)
    span_rows = lax.all_gather(normed, "tp", axis=0, tiled=True)
    gate = jnp.dot(
        span_rows,
        lax.all_gather(gate_weight, "sp", axis=0, tiled=True),
        preferred_element_type=jnp.float32,
    )
    upper = jnp.dot(
        span_rows,
        lax.all_gather(up_weight, "sp", axis=0, tiled=True),
        preferred_element_type=jnp.float32,
    )
    hidden = (jax.nn.silu(gate) * upper).astype(jnp.bfloat16)
    partial_out = jnp.dot(
        hidden,
        lax.all_gather(down_weight, "sp", axis=1, tiled=True),
        preferred_element_type=jnp.float32,
    )
    feed = lax.psum_scatter(
        partial_out.astype(jnp.bfloat16), "tp", scatter_dimension=0, tiled=True
    ).astype(jnp.float32)
    return (stream + feed).astype(jnp.bfloat16)


def solution(mesh):
    in_specs = (
        P(("sp", "tp"), None),
        P("sp", "tp"),
        P("sp", "tp"),
        P("sp", "tp"),
        P("sp"),
        P("tp"),
        P("tp", None),
        P(),
        P("sp", "tp"),
        P("sp", "tp"),
        P("tp", "sp"),
    )
    out_specs = P(("sp", "tp"), None)
    return jax.shard_map(
        on_device, mesh=mesh, in_specs=in_specs, out_specs=out_specs, check_vma=False
    )
```

profile of v0, /device:TPU:17, one launch (start us, length us, event | category | flops | bytes accessed | tf_op | source)
XLA Modules:
  0.0 760.3 jit_solution(9639619573280566356)
XLA Ops:
  8.5 3.1 collective-permute-start.4
  12.7 3.1 collective-permute-start.3
  15.9 3.5 collective-permute-done.4
  19.4 2.2 collective-permute-start.6
  21.7 3.3 collective-permute-done.3
  25.1 2.4 collective-permute-start.5
  27.5 7.5 collective-permute-done.6
  36.1 3.2 collective-permute-start.8
  39.3 6.9 collective-permute-done.5
  47.4 3.2 collective-permute-start.7
  50.6 3.5 collective-permute-start
  54.0 38.1 %collective-permute-done = s32[128]{0:T(128)S(1)} collective-permute-done((s32[128]{0:T(128)S(1)}, s32[128]{0:T(128)S(1)}, u32[]{:S(2)}, u32[]{:S(2)}) %collective-permute-start) | collective-permute-done | bytes 544 | tf_op jit(solution)/shard_map/ppermute | solution.py:10
  94.7 2.6 collective-permute-done.1
  97.4 3.2 collective-permute-start.2
  107.0 17.5 %conditional.4 = (f32[128,16,64]{0,2,1:T(8,128)S(1)}, f32[16,128]{1,0:T(8,128)S(1)}) conditional(s32[]{:T(128)} %convert_element_type.66, () %tuple.49, (s32[]{:T(128)}, s32[128]{0:T(128)S(1)}, s32[256]{0:T(256)S(1)}, s32[128]{0:T(128)S(1)}, bf16[256,1024]{0,1:T(8,128)(2,1)S(1)}, /*index=5*/bf16[128,16,64]{0,2,1:T(8,128)(2,1)S(1)}, f32[16]{0:T(128)S(1)}, ...), branch_computations={%region_0.0_spmd, %region_1.5_spmd} | conditional | flops 223449856 | bytes 37884532 | solution.py:56
  111.3 5.9 fusion.53
  119.2 5.2 convolution_bitcast_fusion.1
  124.5 18.4 %conditional.5 = ((f32[128,16,64]{0,2,1:T(8,128)S(1)}, f32[16,128]{1,0:T(8,128)S(1)})) conditional(s32[]{:T(128)} %convert_element_type.65, (f32[128,16,64]{0,2,1:T(8,128)S(1)}, f32[16,128]{1,0:T(8,128)S(1)}) %conditional.4, (s32[]{:T(128)}, s32[128]{0:T(128)S(1)}, s32[256]{0:T(256)S(1)}, s32[128]{0:T(128)S(1)}, bf16[256,1024]{0,1:T(8,128)(2,1)}, ...), branch_computations={%region_5.6_spmd, %region_6.0_spmd} | conditional | flops 224107264 | bytes 40538776 | solution.py:56
  130.0 5.9 fusion.54
  137.9 5.0 fusion.29
  142.9 19.6 %conditional.6 = ((f32[128,16,64]{0,2,1:T(8,128)S(1)}, f32[16,128]{1,0:T(8,128)S(1)})) conditional(s32[]{:T(128)} %convert_element_type.64, (f32[128,16,64]{0,2,1:T(8,128)S(1)}, f32[16,128]{1,0:T(8,128)S(1)}) %get-tuple-element.230, (s32[]{:T(128)}, s32[128]{0:T(128)S(1)}, s32[512]{0:T(512)S(1)}, s32[128]{0:T(128)S(1)}, ...), branch_computations={%region_10.11_spmd.clone, %region_11.15_spmd.clone} | conditional | flops 224107264 | bytes 40540796 | solution.py:56
  148.6 5.9 fusion.55
  157.5 5.0 fusion.41
  162.9 3.7 convolution_convert_fusion.1
  168.4 68.9 %reduce-scatter.3.cloned.1.call-done = bf16[64,2048]{1,0:T(8,128)(2,1)} async-done(((bf16[128,2048]{1,0:T(8,128)(2,1)}), bf16[64,2048]{1,0:T(8,128)(2,1)}) %reduce-scatter.3.cloned.1.call-update) | async-done | bytes 262160 | tf_op jit(solution)/shard_map/reduce_scatter | solution.py:100
  239.6 2.2 all_gather.12
  241.7 139.4 %all-gather.4.cloned.1.call-done = bf16[2048,3072]{1,0:T(8,128)(2,1)} async-done(((bf16[128,3072]{1,0:T(8,128)(2,1)}), bf16[2048,3072]{1,0:T(8,128)(2,1)}) %all-gather.4.cloned.1.call-update) | async-done | bytes 12582928 | tf_op jit(solution)/shard_map/all_gather | solution.py:113
  381.2 6.4 fusion.56
  387.5 145.5 %all-gather.6.cloned.1.call-done = bf16[2048,3072]{1,0:T(8,128)(2,1)} async-done(((bf16[128,3072]{1,0:T(8,128)(2,1)}), bf16[2048,3072]{1,0:T(8,128)(2,1)}) %all-gather.6.cloned.1.call-update) | async-done | bytes 12582928 | tf_op jit(solution)/shard_map/all_gather | solution.py:118
  533.1 196.1 %all-gather.8.cloned.1.call-done = bf16[3072,2048]{1,0:T(8,128)(2,1)} async-done(((bf16[3072,128]{1,0:T(8,128)(2,1)}), bf16[3072,2048]{1,0:T(8,128)(2,1)}) %all-gather.8.cloned.1.call-update) | async-done | bytes 12582928 | tf_op jit(solution)/shard_map/all_gather | solution.py:124
  729.1 12.7 %convolution_convert_fusion = bf16[128,2048]{1,0:T(8,128)(2,1)} fusion(bf16[3072,2048]{1,0:T(8,128)(2,1)} %all-gather.8.cloned.1.call-done, bf16[128,2048]{1,0:T(8,128)(2,1)S(1)} %all_gather.12, bf16[2048,3072]{1,0:T(8,128)(2,1)} %all-gather.6.cloned.1.call-done, f32[128,3072]{1,0:T(8,128)S(1)} %fusion.56), kind=kOutput, calls=%fused_computation.87 | convolution fusion | flops 3223846912 | bytes 27787264 | tf_op jit(solution)/shard_map/dot_general | solution.py:122
  741.9 8.7 %reduce-scatter.5.cloned.1.call-done = bf16[64,2048]{1,0:T(8,128)(2,1)} async-done(((bf16[128,2048]{1,0:T(8,128)(2,1)}), bf16[64,2048]{1,0:T(8,128)(2,1)}) %reduce-scatter.5.cloned.1.call-update) | async-done | bytes 262160 | tf_op jit(solution)/shard_map/reduce_scatter | solution.py:127
  (94 shorter events, 36.7 us)
Async XLA Ops:
  7.4 230.0 %reduce-scatter.3.cloned.1.call-start = ((), (), s32[]{:S(2)}) async-start(), calls=%async_computation.2 | async-start | bytes 786432 | tf_op jit(solution)/shard_map/reduce_scatter | solution.py:100
  8.5 10.9 %collective-permute-start.4 = (bf16[128,1024]{0,1:T(8,128)(2,1)S(1)}, bf16[128,1024]{0,1:T(8,128)(2,1)S(1)}, u32[]{:S(2)}, u32[]{:S(2)}) collective-permute-start(bf16[128,1024]{0,1:T(8,128)(2,1)S(1)} %copy.23), channel_id=1, source_target_pairs={{0,2},{2,4},{4,6},{6,8},{8,10},{10,12},{12,14},{14,16},{16,18},{18... | collective-permute-start | bytes 786440 | tf_op jit(solution)/shard_map/ppermute | solution.py:10
  12.7 12.2 %collective-permute-start.3 = (bf16[128,1024]{0,1:T(8,128)(2,1)S(1)}, bf16[128,1024]{0,1:T(8,128)(2,1)S(1)}, u32[]{:S(2)}, u32[]{:S(2)}) collective-permute-start(bf16[128,1024]{0,1:T(8,128)(2,1)S(1)} %copy.20), channel_id=1, source_target_pairs={{0,2},{2,4},{4,6},{6,8},{8,10},{10,12},{12,14},{14,16},{16,18},{18... | collective-permute-start | bytes 786440 | tf_op jit(solution)/shard_map/ppermute | solution.py:10
  19.4 15.5 %collective-permute-start.6 = (bf16[256,1024]{0,1:T(8,128)(2,1)S(1)}, bf16[256,1024]{0,1:T(8,128)(2,1)S(1)}, u32[]{:S(2)}, u32[]{:S(2)}) collective-permute-start(bf16[256,1024]{0,1:T(8,128)(2,1)S(1)} %pad_maximum_fusion.3), channel_id=1, source_target_pairs={{0,4},{2,6},{4,8},{6,10},{8,12},{10,14},{12,16},{14,18},{16,20},{1... | collective-permute-start | bytes 1572872 | tf_op jit(solution)/shard_map/ppermute | solution.py:10
  25.1 25.5 %copy-start.9 = (s32[128]{0:T(128)S(1)}, s32[128]{0:T(128)}, u32[]{:S(2)}) copy-start(s32[128]{0:T(128)} %param.23) | copy-start | bytes 1540
  25.1 75.5 %copy-start.8 = (bf16[128,1024]{1,0:T(8,128)(2,1)S(1)}, bf16[128,1024]{1,0:T(8,128)(2,1)}, u32[]{:S(2)}) copy-start(bf16[128,1024]{1,0:T(8,128)(2,1)} %param.20) | copy-start | bytes 786436
  25.1 81.9 %copy-start.11 = (f32[16]{0:T(128)S(1)}, f32[16]{0:T(128)}, u32[]{:S(2)}) copy-start(f32[16]{0:T(128)} %param.24) | copy-start | bytes 196
  25.1 21.1 %collective-permute-start.5 = (bf16[256,1024]{0,1:T(8,128)(2,1)S(1)}, bf16[256,1024]{0,1:T(8,128)(2,1)S(1)}, u32[]{:S(2)}, u32[]{:S(2)}) collective-permute-start(bf16[256,1024]{0,1:T(8,128)(2,1)S(1)} %pad_maximum_fusion.2), channel_id=1, source_target_pairs={{0,4},{2,6},{4,8},{6,10},{8,12},{10,14},{12,16},{14,18},{16,20},{1... | collective-permute-start | bytes 1572872 | tf_op jit(solution)/shard_map/ppermute | solution.py:10
  35.0 12.4 %copy-start.5 = (bf16[256,1024]{0,1:T(8,128)(2,1)}, bf16[256,1024]{0,1:T(8,128)(2,1)S(1)}, u32[]{:S(2)}) copy-start(bf16[256,1024]{0,1:T(8,128)(2,1)S(1)} %collective-permute-done.6) | copy-start | bytes 1572868
  36.1 106.8 %collective-permute-start.8 = (bf16[512,1024]{0,1:T(8,128)(2,1)}, bf16[512,1024]{0,1:T(8,128)(2,1)}, u32[]{:S(2)}, u32[]{:S(2)}) collective-permute-start(bf16[512,1024]{0,1:T(8,128)(2,1)} %pad_maximum_fusion.1), channel_id=1, source_target_pairs={{0,8},{2,10},{4,12},{6,14},{8,16},{10,18},{12,20},{14,22},{16,24},... | collective-permute-start | bytes 3145736 | tf_op jit(solution)/shard_map/ppermute | solution.py:10
  46.2 60.8 %copy-start.7 = (bf16[256,1024]{0,1:T(8,128)(2,1)}, bf16[256,1024]{0,1:T(8,128)(2,1)S(1)}, u32[]{:S(2)}) copy-start(bf16[256,1024]{0,1:T(8,128)(2,1)S(1)} %collective-permute-done.5) | copy-start | bytes 1572868
  47.4 95.6 %collective-permute-start.7 = (bf16[512,1024]{0,1:T(8,128)(2,1)}, bf16[512,1024]{0,1:T(8,128)(2,1)}, u32[]{:S(2)}, u32[]{:S(2)}) collective-permute-start(bf16[512,1024]{0,1:T(8,128)(2,1)} %pad_maximum_fusion), channel_id=1, source_target_pairs={{0,8},{2,10},{4,12},{6,14},{8,16},{10,18},{12,20},{14,22},{16,24},... | collective-permute-start | bytes 3145736 | tf_op jit(solution)/shard_map/ppermute | solution.py:10
  50.6 41.6 %collective-permute-start = (s32[128]{0:T(128)S(1)}, s32[128]{0:T(128)S(1)}, u32[]{:S(2)}, u32[]{:S(2)}) collective-permute-start(s32[128]{0:T(128)S(1)} %copy-done.9), channel_id=1, source_target_pairs={{0,2},{2,4},{4,6},{6,8},{8,10},{10,12},{12,14},{14,16},{16,18},{18... | collective-permute-start | bytes 1544 | tf_op jit(solution)/shard_map/ppermute | solution.py:10
  92.2 5.2 collective-permute-start.1
  97.4 6.5 collective-permute-start.2
  107.8 1.5 copy-start.4
  126.5 1.5 copy-start.3
  136.1 1.8 copy-start.6
  145.1 1.5 copy-start.2
  166.6 70.7 %copy-start = (bf16[64,2048]{1,0:T(8,128)(2,1)S(1)}, bf16[64,2048]{1,0:T(8,128)(2,1)}, u32[]{:S(2)}) copy-start(bf16[64,2048]{1,0:T(8,128)(2,1)} %param.19) | copy-start | bytes 786436
  166.6 71.9 %copy-start.10 = (f32[2048]{0:T(1024)S(1)}, f32[2048]{0:T(1024)}, u32[]{:S(2)}) copy-start(f32[2048]{0:T(1024)} %param.26) | copy-start | bytes 24580
  166.6 214.5 %all-gather.4.cloned.1.call-start = ((), (), s32[]{:S(2)}) async-start(), calls=%async_computation.3 | async-start | bytes 13369344 | tf_op jit(solution)/shard_map/all_gather | solution.py:113
  167.2 365.9 %all-gather.6.cloned.1.call-start = ((), (), s32[]{:S(2)}) async-start(), calls=%async_computation.4 | async-start | bytes 13369344 | tf_op jit(solution)/shard_map/all_gather | solution.py:118
  167.8 561.4 %all-gather.8.cloned.1.call-start = ((), (), s32[]{:S(2)}) async-start(), calls=%async_computation.5 | async-start | bytes 13369344 | tf_op jit(solution)/shard_map/all_gather | solution.py:124
  168.4 582.2 %reduce-scatter.5.cloned.1.call-start = ((), (), s32[]{:S(2)}) async-start(), calls=%async_computation.6 | async-start | bytes 786432 | tf_op jit(solution)/shard_map/reduce_scatter | solution.py:127
  387.5 363.0 %copy-start.1 = (bf16[64,2048]{1,0:T(8,128)(2,1)S(1)}, bf16[64,2048]{1,0:T(8,128)(2,1)}, u32[]{:S(2)}) copy-start(bf16[64,2048]{1,0:T(8,128)(2,1)} %reduce-scatter.3.cloned.1.call-done) | copy-start | bytes 786436
Sparse Core Ops, SparseCore 0:
  166.7 70.5 reduce-scatter.2
  742.0 8.5 reduce-scatter.4
Sparse Core Ops, SparseCore 1:
  169.9 211.2 all-gather.3
  383.8 149.2 all-gather.5
  535.7 193.4 all-gather.7
where the time goes:
time: 771 us; the launch traced here: 760 us
  waiting for transfers between devices  622 us (81%)
  matrix products  41.1 us (5%)
  other arithmetic  29.4 us (4%)
  starting transfers between devices  26 us (3%)
  between operations  20.7 us (3%)
  local copies, waits for them, and re-layouts  17.9 us (2%)
    all_gather x1, waiting for transfers between devices, on_device(): lax.all_gather(down_weight, 'sp', axis=1, tiled=True)  196 us
    all_gather x1, waiting for transfers between devices, on_device(): lax.all_gather(up_weight, 'sp', axis=0, tiled=True)  146 us
    all_gather x1, waiting for transfers between devices, on_device(): lax.all_gather(gate_weight, 'sp', axis=0, tiled=True)  139 us
    reduce_scatter x1, waiting for transfers between devices, on_device(): lax.psum_scatter(jnp.dot(attended, out_weight, preferred_element_type=jnp...  68.9 us
    ppermute x9, waiting for transfers between devices, from_behind(): return lax.ppermute(shard, axis, pairs)  61.9 us
    ppermute x9, starting transfers between devices, from_behind(): return lax.ppermute(shard, axis, pairs)  25.8 us
    another operation x6, other arithmetic  17.7 us
  transfers between devices with their start and end apart: 14, of which 11 were waited for; matrix products, arithmetic and copies ran while one was open for 7% of the time, Pallas kernels for 0%

commit v1 on v0

--- a/solution.py
+++ b/solution.py
@@ -1,6 +1,10 @@
+import functools
+
 import jax
 import jax.numpy as jnp
 from jax import lax
+from jax.experimental import pallas as pl
+from jax.experimental.pallas import tpu as pltpu
 from jax.sharding import PartitionSpec as P
 
 
@@ -56,7 +60,7 @@
     return lax.cond(reached, compute, lambda: carry)
 
 
-def on_device(
+def windowed(
     resid,
     queries,
     keys,
@@ -130,6 +134,294 @@
     return (stream + feed).astype(jnp.bfloat16)
 
 
+DOC_MOST = 896
+MESH = pl.DeviceIdType.MESH
+
+
+def sends(src, dst, send, recv, target):
+    return pltpu.make_async_remote_copy(
+        src_ref=src, dst_ref=dst, send_sem=send, recv_sem=recv, device_id=target, device_id_type=MESH
+    )
+
+
+def head_kernel(
+    n,
+    q_ref, k_ref, v_ref, doc_ref, off_ref, g_in, u_in, d_in,
+    att_ref, wg, wu, wd,
+    sbuf, rbuf, docr, ao,
+    qkv_s, qkv_r, doc_s, doc_r, att_s, att_r, w_s, w_r, f_s, own_sem,
+):
+    s = lax.axis_index("sp")
+    c = lax.axis_index("tp")
+    rows = q_ref.shape[0]
+    half = rows // 2
+    dim = q_ref.shape[1] // n
+    ntp = wg.shape[1] * n // g_in.shape[1]
+    per = n // ntp
+    width = wg.shape[1]
+    depth = g_in.shape[0]
+    dcols = d_in.shape[1]
+    back = -(-DOC_MOST // rows)
+    other = 1 - c
+
+    for j in range(n // 2):
+        cols = slice(j * 2 * dim, (j + 1) * 2 * dim)
+        kp, vp, qp = (r[:, cols].astype(jnp.float32) for r in (k_ref, v_ref, q_ref))
+        low = lax.broadcasted_iota(jnp.int32, (rows, 2 * dim), 1) < dim
+        lowh = low[:half]
+        top, bot = qp[:half], qp[half:]
+        sbuf[2 * j, :rows, :] = jnp.where(low, kp, pltpu.roll(vp, dim, 1)).astype(jnp.bfloat16)
+        sbuf[2 * j + 1, :rows, :] = jnp.where(low, pltpu.roll(kp, dim, 1), vp).astype(jnp.bfloat16)
+        sbuf[2 * j, rows:, :] = jnp.where(lowh, top, pltpu.roll(bot, dim, 1)).astype(jnp.bfloat16)
+        sbuf[2 * j + 1, rows:, :] = jnp.where(lowh, pltpu.roll(top, dim, 1), bot).astype(jnp.bfloat16)
+
+    def qkv_copy(t, src):
+        return sends(sbuf.at[t], rbuf.at[src], qkv_s.at[t], qkv_r.at[src], {"sp": t})
+
+    def doc_copy(t, src):
+        return sends(doc_ref, docr.at[src], doc_s.at[t], doc_r.at[src], {"sp": t})
+
+    def start_peer(k, _):
+        t = lax.rem(s + k, n)
+        qkv_copy(t, s).start()
+        doc_copy(t, s).start()
+        return 0
+
+    lax.fori_loop(1, n, start_peer, 0)
+    rbuf[pl.ds(s, 1)] = sbuf[pl.ds(s, 1)]
+    docr[pl.ds(s, 1)] = doc_ref[...][None]
+
+    tc = lax.rem(s, 2)
+    mats = ((g_in, wg), (u_in, wu), (d_in, wd))
+
+    def part_of(m, p):
+        start = pl.multiple_of((p - per * c) * width, width)
+        return mats[m][0].at[pl.ds(start, width), :] if m == 2 else mats[m][0].at[:, pl.ds(start, width)]
+
+    def slot_of(m, src):
+        if m == 2:
+            return mats[m][1].at[:, pl.ds(pl.multiple_of(src * dcols, dcols), dcols)]
+        return mats[m][1].at[pl.ds(pl.multiple_of(src * depth, depth), depth), :]
+
+    def w_copy(m, p, k):
+        return sends(part_of(m, p), slot_of(m, s), w_s.at[m, k], w_r.at[m, s], {"sp": p, "tp": tc})
+
+    def own_copy(m, p):
+        return pltpu.make_async_copy(part_of(m, p), slot_of(m, s), own_sem.at[m])
+
+    for m in range(3):
+
+        def start_weight(k, _, m=m):
+            p = per * c + lax.rem(s + k, per)
+            mine = (p == s) & (tc == c)
+
+            @pl.when(mine)
+            def _():
+                own_copy(m, p).start()
+
+            @pl.when(jnp.logical_not(mine))
+            def _():
+                w_copy(m, p, k).start()
+
+            return 0
+
+        lax.fori_loop(0, per, start_weight, 0)
+
+    def wait_peer(k, _):
+        src = lax.rem(s + n - k, n)
+        qkv_copy(src, src).wait_recv()
+        doc_copy(src, src).wait_recv()
+        return 0
+
+    lax.fori_loop(1, n, wait_peer, 0)
+
+    scale = dim ** (-0.5)
+    off = off_ref[s]
+    lane = lax.broadcasted_iota(jnp.int32, (half, 2 * dim), 1) < dim
+    row_i = lax.broadcasted_iota(jnp.int32, (rows, rows), 0)
+    col_i = lax.broadcasted_iota(jnp.int32, (rows, rows), 1)
+    later = (row_i > col_i).astype(jnp.bfloat16)
+    nt = (((1,), (1,)), ((), ()))
+
+    def att_copy(t, src):
+        return sends(ao.at[t], att_ref.at[src], att_s.at[t], att_r.at[src], {"sp": t})
+
+    def block(step, _):
+        i = lax.rem(s + step, n)
+        q2 = rbuf[i, rows:, :].astype(jnp.float32)
+        q_pad = jnp.concatenate(
+            [jnp.where(lane, q2, 0.0), jnp.where(lane, pltpu.roll(q2, dim, 1), 0.0)], axis=0
+        ).astype(jnp.bfloat16)
+        q_doc = jnp.broadcast_to(docr[i, 0:1, :].astype(jnp.float32), (rows, rows)).T
+        total = jnp.zeros((rows, 2 * dim), jnp.float32)
+        carried = jnp.zeros((rows, 1), jnp.float32)
+        for d in range(min(back, n - 1) + 1):
+            j = jnp.maximum(i - d, 0)
+            kv = rbuf[j, :rows, :]
+            k_doc = jnp.where(i >= d, docr[j, 0:1, :].astype(jnp.float32), -1.0)
+            z = lax.dot_general(q_pad, kv, nt, preferred_element_type=jnp.float32) * scale + off
+            live = q_doc == k_doc
+            if d == 0:
+                live = live & (col_i < row_i)
+            soft = jnp.log(1.0 + jnp.exp(-jnp.abs(z)))
+            keep = jnp.where(live, -jnp.maximum(z, 0.0) - soft, 0.0)
+            high = keep.astype(jnp.bfloat16)
+            rest = (keep - high.astype(jnp.float32)).astype(jnp.bfloat16)
+            tail = jnp.dot(high, later, preferred_element_type=jnp.float32) + jnp.dot(
+                rest, later, preferred_element_type=jnp.float32
+            )
+            weight = jnp.where(
+                live, jnp.exp(jnp.minimum(z, 0.0) - soft + (tail + carried)), 0.0
+            ).astype(jnp.bfloat16)
+            total = total + jnp.dot(weight, kv, preferred_element_type=jnp.float32)
+            carried = carried + jnp.sum(keep, axis=1, keepdims=True)
+        packed = jnp.where(lane, pltpu.roll(total[:half], dim, 1), total[half:]).astype(jnp.bfloat16)
+
+        @pl.when(i == s)
+        def _():
+            att_ref[pl.ds(s, 1)] = packed[None]
+
+        @pl.when(i != s)
+        def _():
+            ao[pl.ds(i, 1)] = packed[None]
+            att_copy(i, s).start()
+
+        return 0
+
+    lax.fori_loop(0, n, block, 0)
+
+    def forward(m, src, k):
+        return sends(slot_of(m, src), slot_of(m, src), f_s.at[m, k], w_r.at[m, src], {"tp": other})
+
+    base_c = s // per
+    for m in range(3):
+
+        def pass_on(k, _, m=m):
+            src = 2 * k + c
+            mine = (src == s) & (base_c == c)
+
+            @pl.when(mine)
+            def _():
+                own_copy(m, s).wait()
+
+            @pl.when(jnp.logical_not(mine))
+            def _():
+                forward(m, src, k).wait_recv()
+
+            forward(m, src, k).start()
+            return 0
+
+        lax.fori_loop(0, n // 2, pass_on, 0)
+
+    def finish_peer(k, _):
+        src = lax.rem(s + n - k, n)
+        att_copy(src, src).wait_recv()
+        att_copy(src, src).wait_send()
+        qkv_copy(src, src).wait_send()
+        doc_copy(src, src).wait_send()
+        return 0
+
+    lax.fori_loop(1, n, finish_peer, 0)
+    for m in range(3):
+
+        def finish_forward(k, _, m=m):
+            forward(m, 2 * k + other, k).wait_recv()
+            forward(m, 2 * k + c, k).wait_send()
+            return 0
+
+        lax.fori_loop(0, n // 2, finish_forward, 0)
+
+        def finish_weight(k, _, m=m):
+            p = per * c + lax.rem(s + k, per)
+
+            @pl.when(jnp.logical_not((p == s) & (tc == c)))
+            def _():
+                w_copy(m, p, k).wait_send()
+
+            return 0
+
+        lax.fori_loop(0, per, finish_weight, 0)
+
+
+def heads_and_weights(n, ntp, queries, keys, values, doc_ids, score_offset, gate_weight, up_weight, down_weight):
+    rows, local = queries.shape
+    half, two = rows // 2, 2 * (local // n)
+    d_model = n * gate_weight.shape[0]
+    width = gate_weight.shape[1] * ntp // n
+    bf = jnp.bfloat16
+    vmem = pl.BlockSpec(memory_space=pltpu.VMEM)
+    anyw = pl.BlockSpec(memory_space=pl.ANY)
+    dma = pltpu.SemaphoreType.DMA
+    per = n // ntp
+    return pl.pallas_call(
+        functools.partial(head_kernel, n),
+        out_shape=(
+            jax.ShapeDtypeStruct((n, half, two), bf),
+            jax.ShapeDtypeStruct((d_model, width), bf),
+            jax.ShapeDtypeStruct((d_model, width), bf),
+            jax.ShapeDtypeStruct((width, d_model), bf),
+        ),
+        in_specs=[vmem] * 4 + [pl.BlockSpec(memory_space=pltpu.SMEM)] + [anyw] * 3,
+        out_specs=(vmem, anyw, anyw, anyw),
+        scratch_shapes=[
+            pltpu.VMEM((n, rows + half, two), bf),
+            pltpu.VMEM((n, rows + half, two), bf),
+            pltpu.VMEM((n, 8, rows), jnp.int32),
+            pltpu.VMEM((n, half, two), bf),
+            dma((n,)), dma((n,)), dma((n,)), dma((n,)), dma((n,)), dma((n,)),
+            dma((3, per)), dma((3, n)), dma((3, n // 2)), dma((3,)),
+        ],
+        compiler_params=pltpu.CompilerParams(has_side_effects=True, vmem_limit_bytes=48 << 20),
+    )(
+        queries, keys, values, jnp.broadcast_to(doc_ids[None], (8, rows)), score_offset,
+        gate_weight, up_weight, down_weight,
+    )
+
+
+def resharded(
+    resid, queries, keys, values, doc_ids, score_offset, out_weight, norm_gain,
+    gate_weight, up_weight, down_weight,
+):
+    n, ntp = lax.axis_size("sp"), lax.axis_size("tp")
+    rows, local = queries.shape
+    half, dim = rows // 2, local // n
+    att, wg, wu, wd = heads_and_weights(
+        n, ntp, queries, keys, values, doc_ids, score_offset, gate_weight, up_weight, down_weight
+    )
+    attended = att.reshape(n, half, 2, dim).transpose(2, 1, 0, 3).reshape(rows, local)
+    mixed_attn = lax.psum_scatter(
+        jnp.dot(attended, out_weight, preferred_element_type=jnp.float32).astype(jnp.bfloat16),
+        "tp", scatter_dimension=0, tiled=True,
+    ).astype(jnp.float32)
+    stream = resid.astype(jnp.float32) + mixed_attn
+    normed = (
+        stream * lax.rsqrt(jnp.mean(stream * stream, axis=1, keepdims=True) + 1e-06) * norm_gain
+    ).astype(jnp.bfloat16)
+    every = lax.all_gather(normed, "sp", axis=0, tiled=True)
+    gate = jnp.dot(every, wg, preferred_element_type=jnp.float32)
+    upper = jnp.dot(every, wu, preferred_element_type=jnp.float32)
+    hidden = (jax.nn.silu(gate) * upper).astype(jnp.bfloat16)
+    partial_out = jnp.dot(hidden, wd, preferred_element_type=jnp.float32).astype(jnp.bfloat16)
+    feed = lax.psum_scatter(partial_out, "sp", scatter_dimension=0, tiled=True)
+    return (stream + feed.astype(jnp.float32)).astype(jnp.bfloat16)
+
+
+def on_device(*args):
+    queries, doc_ids, score_offset, gate_weight = args[1], args[4], args[5], args[8]
+    n, ntp = lax.axis_size("sp"), lax.axis_size("tp")
+    dim = queries.shape[1] // score_offset.shape[0]
+    fits = (
+        ntp == 2
+        and score_offset.shape[0] == n
+        and 2 * dim == 128
+        and doc_ids.shape[0] == 128
+        and n % 2 == 0
+        and gate_weight.shape[1] * ntp % (n * 128) == 0
+        and gate_weight.shape[0] % 128 == 0
+    )
+    return resharded(*args) if fits else windowed(*args)
+
+
 def solution(mesh):
     in_specs = (
         P(("sp", "tp"), None),

time: 771 us -> 312 us (0.40)
  waiting for transfers between devices: 622 us -> 177 us
  Pallas kernels: 0 us -> 86.1 us
  starting transfers between devices: 26 us -> 0.09 us
  other arithmetic: 29.4 us -> 4.66 us
  matrix products: 41.1 us -> 17.9 us
  local copies, waits for them, and re-layouts: 17.9 us -> 8.5 us
    all_gather x3 -> x1, waiting for transfers between devices: 481 us -> 74.9 us  [resharded(): every = lax.all_gather(normed, 'sp', axis=0, tiled=True)]
    pallas_call x0 -> x1, Pallas kernels: none -> 86.1 us  [heads_and_weights(): pl.pallas_call(functools.partial(head_kernel, n), out_shape=(jax.ShapeDty...]
    ppermute x9 -> x0, waiting for transfers between devices: 61.9 us -> none  [from_behind(): return lax.ppermute(shard, axis, pairs)]
    ppermute x9 -> x0, starting transfers between devices: 25.8 us -> none  [from_behind(): return lax.ppermute(shard, axis, pairs)]
    reduce_scatter x2, waiting for transfers between devices: 77.6 us -> 102 us  [the longest x1 92.5 us: resharded(): feed = lax.psum_scatter(partial_out, 'sp', scatter_dimension=0, tiled=True)]
    dot_general x9 -> x3, matrix products: 41.1 us -> 17.9 us  [the longest x1 8.33 us: resharded(): jnp.dot(hidden, wd, preferred_element_type=jnp.float32).astype(jnp.bfloat16)]
    another operation x9 -> x0, other arithmetic: 18.1 us -> none
    another operation x8 -> x0, local copies, waits for them, and re-layouts: 9.43 us -> none  [the longest x3 5.48 us: compute(): lax.cumsum(log_keep, axis=2, reverse=True) - log_keep + carried[:, :, None]]
  transfers between devices with their start and end apart: 14 -> 3, of which waited for: 11 -> 3; matrix products, arithmetic and copies ran while one was open for 7% -> 0% of each run, Pallas kernels for 0% -> 0%
where the time goes in v1:
time: 312 us; the launch traced here: 307 us
  waiting for transfers between devices  177 us (57%)
  Pallas kernels  86.1 us (28%)
  matrix products  17.9 us (6%)
  between operations  13.2 us (4%)
  local copies, waits for them, and re-layouts  8.5 us (3%)
  other arithmetic  4.66 us (1%)
    reduce_scatter x1, waiting for transfers between devices, resharded(): feed = lax.psum_scatter(partial_out, 'sp', scatter_dimension=0, tiled=True)  92.5 us
    pallas_call x1, Pallas kernels, heads_and_weights(): pl.pallas_call(functools.partial(head_kernel, n), out_shape=(jax.ShapeDty...  86.1 us
    all_gather x1, waiting for transfers between devices, resharded(): every = lax.all_gather(normed, 'sp', axis=0, tiled=True)  74.9 us
    reduce_scatter x1, waiting for transfers between devices, resharded(): lax.psum_scatter(jnp.dot(attended, out_weight, preferred_element_type=jnp...  9.18 us
    dot_general x1, matrix products, resharded(): jnp.dot(hidden, wd, preferred_element_type=jnp.float32).astype(jnp.bfloat16)  8.33 us
    unnamed x22, local copies, waits for them, and re-layouts  6.92 us
  transfers between devices with their start and end apart: 3, of which 3 were waited for; matrix products, arithmetic and copies ran while one was open for 0% of the time, Pallas kernels for 0%

profile of v1, /device:TPU:17, one launch (start us, length us, event | category | flops | bytes accessed | tf_op | source)
XLA Modules:
  0.0 307.0 jit_solution(2466758065326700354)
XLA Ops:
  6.5 0.0 reduce-scatter.3.cloned.1.call-start
  6.5 0.7 broadcast_in_dim.2.doc_ref
  7.2 1.1 copy-done
  8.3 1.1 copy-done.1
  9.5 1.1 copy-done.2
  10.6 0.9 copy-done.3
  11.5 0.9 copy-done.4
  12.5 0.9 copy-done.5
  13.4 0.7 copy-done.6
  14.1 86.1 %shard_map.109 = (bf16[16,64,128]{2,1,0:T(8,128)(2,1)S(1)}, bf16[2048,384]{1,0:T(8,128)(2,1)S(1)}, bf16[2048,384]{1,0:T(8,128)(2,1)}, bf16[384,2048]{1,0:T(8,128)(2,1)}) custom-call(bf16[128,1024]{1,0:T(8,128)(2,1)S(1)} %copy-done.3, bf16[128,1024]{1,0:T(8,128)(2,1)S(1)} %copy-done.4, bf16[128,1024]{1,0:T(8,128)(2,1)S(1)} %copy-done.5, ...), custom_call_target="tpu_custom_call" | custom-call | tf_op jit(solution)/shard_map/pallas_call | solution.py:356
  100.2 0.2 reshape.16
  100.4 0.3 copy.14
  100.8 0.3 reshape.17
  101.1 0.0 copy-start.7
  101.2 0.0 copy-start.9
  101.2 3.7 %convolution_convert_fusion.1 = bf16[128,2048]{1,0:T(8,128)(2,1)} fusion(bf16[128,1024]{1,0:T(8,128)(2,1)S(1)} %reshape.17, bf16[1024,2048]{1,0:T(8,128)(2,1)} %param.17), kind=kOutput, calls=%fused_computation.1 | convolution fusion | flops 537133056 | bytes 4980736 | tf_op jit(solution)/shard_map/dot_general | solution.py:393
  104.9 0.0 reduce-scatter.3.cloned.1.call-update
  104.9 0.0 all-gather.2.cloned.1.call-start
  105.0 9.2 %reduce-scatter.3.cloned.1.call-done = bf16[64,2048]{1,0:T(8,128)(2,1)} async-done(((bf16[128,2048]{1,0:T(8,128)(2,1)}), bf16[64,2048]{1,0:T(8,128)(2,1)}) %reduce-scatter.3.cloned.1.call-update) | async-done | bytes 262160 | tf_op jit(solution)/shard_map/reduce_scatter | solution.py:392
  114.2 0.0 copy-done.7
  114.2 1.1 multiply_reduce_fusion
  115.3 0.0 copy-done.9
  115.3 1.8 multiply_convert_fusion.1
  117.1 0.0 all-gather.2.cloned.1.call-update
  117.1 0.0 reduce-scatter.5.cloned.1.call-start
  117.2 74.9 %all-gather.2.cloned.1.call-done = bf16[1024,2048]{1,0:T(8,128)(2,1)} async-done(((bf16[64,2048]{1,0:T(8,128)(2,1)}), bf16[1024,2048]{1,0:T(8,128)(2,1)}) %all-gather.2.cloned.1.call-update) | async-done | bytes 4194320 | tf_op jit(solution)/shard_map/all_gather | solution.py:400
  192.1 5.8 %fusion.1 = f32[1024,384]{1,0:T(8,128)} fusion(bf16[1024,2048]{1,0:T(8,128)(2,1)} %all-gather.2.cloned.1.call-done, bf16[2048,384]{1,0:T(8,128)(2,1)S(1)} %get-tuple-element.10), kind=kOutput, calls=%fused_computation.10 | convolution fusion | flops 1610612736 | bytes 7340032 | tf_op jit(solution)/shard_map/dot_general | solution.py:401
  197.8 0.0 copy-done.10
  197.8 8.3 %convolution_convert_fusion = bf16[1024,2048]{1,0:T(8,128)(2,1)} fusion(bf16[384,2048]{1,0:T(8,128)(2,1)} %get-tuple-element.12, f32[1024,384]{1,0:T(8,128)} %fusion.1, bf16[1024,2048]{1,0:T(8,128)(2,1)} %all-gather.2.cloned.1.call-done, bf16[2048,384]{1,0:T(8,128)(2,1)S(1)} %copy-done.10), kind=kOutput, calls=%fused_computation | convolution fusion | flops 3225681920 | bytes 13107200 | tf_op jit(solution)/shard_map/dot_general | solution.py:404
  206.2 0.0 reduce-scatter.5.cloned.1.call-update
  206.2 92.5 %reduce-scatter.5.cloned.1.call-done = bf16[64,2048]{1,0:T(8,128)(2,1)} async-done(((bf16[1024,2048]{1,0:T(8,128)(2,1)}), bf16[64,2048]{1,0:T(8,128)(2,1)}) %reduce-scatter.5.cloned.1.call-update) | async-done | bytes 262160 | tf_op jit(solution)/shard_map/reduce_scatter | solution.py:405
  298.7 1.7 add_convert_fusion
  (11 shorter events, 0.0 us)
Async XLA Ops:
  6.5 107.6 %reduce-scatter.3.cloned.1.call-start = ((), (), s32[]{:S(2)}) async-start(), calls=%async_computation.2 | async-start | bytes 786432 | tf_op jit(solution)/shard_map/reduce_scatter | solution.py:392
  7.2 1.1 copy-start
  8.3 1.1 copy-start.1
  9.5 1.1 copy-start.2
  10.6 0.9 copy-start.3
  11.5 0.9 copy-start.4
  12.5 0.9 copy-start.5
  13.4 0.7 copy-start.6
  101.1 13.0 %copy-start.7 = (bf16[64,2048]{1,0:T(8,128)(2,1)S(1)}, bf16[64,2048]{1,0:T(8,128)(2,1)}, u32[]{:S(2)}) copy-start(bf16[64,2048]{1,0:T(8,128)(2,1)} %param.11) | copy-start | bytes 786436
  101.2 14.2 %copy-start.9 = (f32[2048]{0:T(1024)S(1)}, f32[2048]{0:T(1024)}, u32[]{:S(2)}) copy-start(f32[2048]{0:T(1024)} %param.18) | copy-start | bytes 24580
  104.9 87.1 %all-gather.2.cloned.1.call-start = ((), (), s32[]{:S(2)}) async-start(), calls=%async_computation.3 | async-start | bytes 4456448 | tf_op jit(solution)/shard_map/all_gather | solution.py:400
  117.1 181.6 %reduce-scatter.5.cloned.1.call-start = ((), (), s32[]{:S(2)}) async-start(), calls=%async_computation.4 | async-start | bytes 4456448 | tf_op jit(solution)/shard_map/reduce_scatter | solution.py:405
  192.1 5.8 %copy-start.10 = (bf16[2048,384]{1,0:T(8,128)(2,1)S(1)}, bf16[2048,384]{1,0:T(8,128)(2,1)}, u32[]{:S(2)}) copy-start(bf16[2048,384]{1,0:T(8,128)(2,1)} %get-tuple-element.11) | copy-start | bytes 4718596
  206.2 92.5 %copy-start.8 = (bf16[64,2048]{1,0:T(8,128)(2,1)S(1)}, bf16[64,2048]{1,0:T(8,128)(2,1)}, u32[]{:S(2)}) copy-start(bf16[64,2048]{1,0:T(8,128)(2,1)} %reduce-scatter.3.cloned.1.call-done) | copy-start | bytes 786436
Sparse Core Ops, SparseCore 0:
  105.1 9.0 reduce-scatter.2
  117.2 74.7 all-gather.1
  206.3 92.3 reduce-scatter.4

commit v2 on v1

--- a/solution.py
+++ b/solution.py
@@ -144,12 +144,13 @@
     )
 
 
-def head_kernel(
+def layer_kernel(
     n,
-    q_ref, k_ref, v_ref, doc_ref, off_ref, g_in, u_in, d_in,
-    att_ref, wg, wu, wd,
-    sbuf, rbuf, docr, ao,
-    qkv_s, qkv_r, doc_s, doc_r, att_s, att_r, w_s, w_r, f_s, own_sem,
+    q_ref, k_ref, v_ref, doc_ref, off_ref, g_in, u_in, d_in, resid_ref, gain_ref, o_in,
+    out_ref,
+    sbuf, rbuf, docr, ao, att_ref, wg, wu, wd, ow,
+    attd, mixed, mixed_in, stream, ag, part, xd, yd, fx, fy, zr,
+    qkv_s, qkv_r, doc_s, doc_r, att_s, att_r, w_s, w_r, f_s, own_sem, o_sem, mix_s, mix_r, net_s, net_r,
 ):
     s = lax.axis_index("sp")
     c = lax.axis_index("tp")
@@ -163,6 +164,7 @@
     dcols = d_in.shape[1]
     back = -(-DOC_MOST // rows)
     other = 1 - c
+    pltpu.make_async_copy(o_in, ow, o_sem).start()
 
     for j in range(n // 2):
         cols = slice(j * 2 * dim, (j + 1) * 2 * dim)
@@ -290,6 +292,153 @@
 
     lax.fori_loop(0, n, block, 0)
 
+    def wait_attended(k, _):
+        src = lax.rem(s + n - k, n)
+        att_copy(src, src).wait_recv()
+        return 0
+
+    lax.fori_loop(1, n, wait_attended, 0)
+    for j in range(n // 2):
+        cols = slice(j * 2 * dim, (j + 1) * 2 * dim)
+        ha, hb = (att_ref[2 * j + e].astype(jnp.float32) for e in range(2))
+        attd[:half, cols] = jnp.where(lane, ha, pltpu.roll(hb, dim, 1)).astype(jnp.bfloat16)
+        attd[half:, cols] = jnp.where(lane, pltpu.roll(ha, dim, 1), hb).astype(jnp.bfloat16)
+
+    pltpu.make_async_copy(o_in, ow, o_sem).wait()
+    dm = ow.shape[1]
+    tile = min(512, dm)
+
+    def project(t, _):
+        cols = pl.ds(pl.multiple_of(t * tile, tile), tile)
+        prod = jnp.dot(attd[...], ow[:, cols], preferred_element_type=jnp.float32).astype(jnp.bfloat16)
+        mixed[0, :, cols] = prod[:half]
+        mixed[1, :, cols] = prod[half:]
+        return 0
+
+    lax.fori_loop(0, dm // tile, project, 0)
+    mix = sends(mixed.at[other], mixed_in, mix_s, mix_r, {"tp": other})
+    mix.start()
+    mix.wait_recv()
+    rows_f = resid_ref[...].astype(jnp.float32) + (
+        mixed[c].astype(jnp.float32) + mixed_in[...].astype(jnp.float32)
+    )
+    stream[...] = rows_f
+    inv = lax.rsqrt(jnp.mean(rows_f * rows_f, axis=1, keepdims=True) + 1e-06)
+    ag[pl.ds(s, 1)] = (rows_f * inv * gain_ref[...]).astype(jnp.bfloat16)[None]
+
+    levels = n // 4
+    quarter = half // 2
+    up, down = slice(0, quarter), slice(quarter, half)
+
+    def flip(v, mask):
+        bit = 1
+        moved = v
+        while bit <= mask:
+            if mask & bit:
+                moved = moved + bit - 2 * bit * lax.rem(lax.div(v, bit), 2)
+            bit *= 2
+        return moved
+
+    xn, yn = flip(s, 1), flip(s, 2)
+
+    def link(kind, k, src, dst, to):
+        return sends(src, dst, net_s.at[kind, k], net_r.at[kind, k], {"sp": to})
+
+    def ids(k):
+        return tuple(flip(s, 4 * k + e) for e in range(4))
+
+    def ag_z(k):
+        return link(0, k, ag.at[s], ag.at[s], ids(k)[0])
+
+    def ag_x(k):
+        return link(1, k, ag.at[ids(k)[0]], ag.at[ids(k)[0]], xn)
+
+    def ag_y(k):
+        return link(2, k, ag.at[ids(k)[0]], ag.at[ids(k)[0]], yn)
+
+    def ag_hx(k):
+        return link(3, k, ag.at[ids(k)[1], up], ag.at[ids(k)[1], up], yn)
+
+    def ag_hy(k):
+        return link(4, k, ag.at[ids(k)[2], down], ag.at[ids(k)[2], down], xn)
+
+    def rs_d1(k):
+        return link(5, k, part.at[ids(k)[3], up], xd.at[k], xn)
+
+    def rs_d2(k):
+        return link(6, k, part.at[ids(k)[3], down], yd.at[k], yn)
+
+    def rs_px(k):
+        return link(7, k, part.at[ids(k)[1], up], fx.at[k, up], xn)
+
+    def rs_qx(k):
+        return link(8, k, part.at[ids(k)[1], down], fx.at[k, down], xn)
+
+    def rs_py(k):
+        return link(9, k, part.at[ids(k)[2], down], fy.at[k, down], yn)
+
+    def rs_qy(k):
+        return link(10, k, part.at[ids(k)[2], up], fy.at[k, up], yn)
+
+    def rs_z(k):
+        return link(11, k, part.at[ids(k)[0]], zr.at[k], ids(k)[0])
+
+    def spread(k):
+        if k > 0:
+            ag_z(k).wait_recv()
+        ag_x(k).start()
+        ag_y(k).start()
+
+    def relay(k):
+        ag_x(k).wait_recv()
+        ag_hx(k).start()
+        ag_y(k).wait_recv()
+        ag_hy(k).start()
+
+    def feed_forward(k):
+        ag_hx(k).wait_recv()
+        ag_hy(k).wait_recv()
+        base = flip(s - lax.rem(s, 4), 4 * k)
+        x = ag[pl.ds(base, 4)].reshape(4 * half, dm)
+        gate = jnp.dot(x, wg[...], preferred_element_type=jnp.float32)
+        upper = jnp.dot(x, wu[...], preferred_element_type=jnp.float32)
+        hidden = (gate / (1.0 + jnp.exp(-gate)) * upper).astype(jnp.bfloat16)
+
+        def columns(t, _):
+            cols = pl.ds(pl.multiple_of(t * tile, tile), tile)
+            prod = jnp.dot(hidden, wd[:, cols], preferred_element_type=jnp.float32)
+            part[pl.ds(base, 4), :, cols] = prod.astype(jnp.bfloat16).reshape(4, half, tile)
+            return 0
+
+        lax.fori_loop(0, dm // tile, columns, 0)
+        for send in (rs_d1, rs_d2, rs_px, rs_py):
+            send(k).start()
+
+    def add_relayed(k):
+        rs_d1(k).wait_recv()
+        at = ids(k)[2]
+        part[at, up] = (part[at, up].astype(jnp.float32) + xd[k].astype(jnp.float32)).astype(jnp.bfloat16)
+        rs_qy(k).start()
+        rs_d2(k).wait_recv()
+        at = ids(k)[1]
+        part[at, down] = (part[at, down].astype(jnp.float32) + yd[k].astype(jnp.float32)).astype(jnp.bfloat16)
+        rs_qx(k).start()
+
+    def collect(k):
+        for send in (rs_px, rs_py, rs_qx, rs_qy):
+            send(k).wait_recv()
+        at = ids(k)[0]
+        summed = part[at].astype(jnp.float32) + fx[k].astype(jnp.float32) + fy[k].astype(jnp.float32)
+        if k == 0:
+            stream[...] = stream[...] + summed
+        else:
+            part[at] = summed.astype(jnp.bfloat16)
+            rs_z(k).start()
+
+    spread(0)
+    for k in range(1, levels):
+        ag_z(k).start()
+
     def forward(m, src, k):
         return sends(slot_of(m, src), slot_of(m, src), f_s.at[m, k], w_r.at[m, src], {"tp": other})
 
@@ -313,9 +462,43 @@
 
         lax.fori_loop(0, n // 2, pass_on, 0)
 
+    for m in range(3):
+
+        def arrived(k, _, m=m):
+            forward(m, 2 * k + other, k).wait_recv()
+            return 0
+
+        lax.fori_loop(0, n // 2, arrived, 0)
+
+    relay(0)
+    for k in range(levels + 2):
+        if k + 1 < levels:
+            spread(k + 1)
+        if k < levels:
+            feed_forward(k)
+        if 1 <= k <= levels:
+            add_relayed(k - 1)
+        if k >= 2:
+            collect(k - 2)
+        if k + 1 < levels:
+            relay(k + 1)
+    for k in range(1, levels):
+        rs_z(k).wait_recv()
+    out = stream[...]
+    for k in range(1, levels):
+        out = out + zr[k].astype(jnp.float32)
+    out_ref[...] = out.astype(jnp.bfloat16)
+
+    mix.wait_send()
+    for k in range(levels):
+        for send in (ag_x, ag_y, ag_hx, ag_hy, rs_d1, rs_d2, rs_px, rs_qx, rs_py, rs_qy):
+            send(k).wait_send()
+        if k > 0:
+            ag_z(k).wait_send()
+            rs_z(k).wait_send()
+
     def finish_peer(k, _):
         src = lax.rem(s + n - k, n)
-        att_copy(src, src).wait_recv()
         att_copy(src, src).wait_send()
         qkv_copy(src, src).wait_send()
         doc_copy(src, src).wait_send()
@@ -325,7 +508,6 @@
     for m in range(3):
 
         def finish_forward(k, _, m=m):
-            forward(m, 2 * k + other, k).wait_recv()
             forward(m, 2 * k + c, k).wait_send()
             return 0
 
@@ -341,41 +523,6 @@
             return 0
 
         lax.fori_loop(0, per, finish_weight, 0)
-
-
-def heads_and_weights(n, ntp, queries, keys, values, doc_ids, score_offset, gate_weight, up_weight, down_weight):
-    rows, local = queries.shape
-    half, two = rows // 2, 2 * (local // n)
-    d_model = n * gate_weight.shape[0]
-    width = gate_weight.shape[1] * ntp // n
-    bf = jnp.bfloat16
-    vmem = pl.BlockSpec(memory_space=pltpu.VMEM)
-    anyw = pl.BlockSpec(memory_space=pl.ANY)
-    dma = pltpu.SemaphoreType.DMA
-    per = n // ntp
-    return pl.pallas_call(
-        functools.partial(head_kernel, n),
-        out_shape=(
-            jax.ShapeDtypeStruct((n, half, two), bf),
-            jax.ShapeDtypeStruct((d_model, width), bf),
-            jax.ShapeDtypeStruct((d_model, width), bf),
-            jax.ShapeDtypeStruct((width, d_model), bf),
-        ),
-        in_specs=[vmem] * 4 + [pl.BlockSpec(memory_space=pltpu.SMEM)] + [anyw] * 3,
-        out_specs=(vmem, anyw, anyw, anyw),
-        scratch_shapes=[
-            pltpu.VMEM((n, rows + half, two), bf),
-            pltpu.VMEM((n, rows + half, two), bf),
-            pltpu.VMEM((n, 8, rows), jnp.int32),
-            pltpu.VMEM((n, half, two), bf),
-            dma((n,)), dma((n,)), dma((n,)), dma((n,)), dma((n,)), dma((n,)),
-            dma((3, per)), dma((3, n)), dma((3, n // 2)), dma((3,)),
-        ],
-        compiler_params=pltpu.CompilerParams(has_side_effects=True, vmem_limit_bytes=48 << 20),
-    )(
-        queries, keys, values, jnp.broadcast_to(doc_ids[None], (8, rows)), score_offset,
-        gate_weight, up_weight, down_weight,
-    )
 
 
 def resharded(
@@ -384,26 +531,51 @@
 ):
     n, ntp = lax.axis_size("sp"), lax.axis_size("tp")
     rows, local = queries.shape
-    half, dim = rows // 2, local // n
-    att, wg, wu, wd = heads_and_weights(
-        n, ntp, queries, keys, values, doc_ids, score_offset, gate_weight, up_weight, down_weight
-    )
-    attended = att.reshape(n, half, 2, dim).transpose(2, 1, 0, 3).reshape(rows, local)
-    mixed_attn = lax.psum_scatter(
-        jnp.dot(attended, out_weight, preferred_element_type=jnp.float32).astype(jnp.bfloat16),
-        "tp", scatter_dimension=0, tiled=True,
-    ).astype(jnp.float32)
-    stream = resid.astype(jnp.float32) + mixed_attn
-    normed = (
-        stream * lax.rsqrt(jnp.mean(stream * stream, axis=1, keepdims=True) + 1e-06) * norm_gain
-    ).astype(jnp.bfloat16)
-    every = lax.all_gather(normed, "sp", axis=0, tiled=True)
-    gate = jnp.dot(every, wg, preferred_element_type=jnp.float32)
-    upper = jnp.dot(every, wu, preferred_element_type=jnp.float32)
-    hidden = (jax.nn.silu(gate) * upper).astype(jnp.bfloat16)
-    partial_out = jnp.dot(hidden, wd, preferred_element_type=jnp.float32).astype(jnp.bfloat16)
-    feed = lax.psum_scatter(partial_out, "sp", scatter_dimension=0, tiled=True)
-    return (stream + feed.astype(jnp.float32)).astype(jnp.bfloat16)
+    half, two = rows // 2, 2 * (local // n)
+    dm = resid.shape[1]
+    width = gate_weight.shape[1] * ntp // n
+    levels = n // 4
+    bf, f32 = jnp.bfloat16, jnp.float32
+    vmem = pl.BlockSpec(memory_space=pltpu.VMEM)
+    anyw = pl.BlockSpec(memory_space=pl.ANY)
+    dma = pltpu.SemaphoreType.DMA
+    per = n // ntp
+    block = (half, dm)
+    return pl.pallas_call(
+        functools.partial(layer_kernel, n),
+        out_shape=jax.ShapeDtypeStruct(block, bf),
+        in_specs=[vmem] * 4 + [pl.BlockSpec(memory_space=pltpu.SMEM)] + [anyw] * 3 + [vmem] * 2 + [anyw],
+        out_specs=vmem,
+        scratch_shapes=[
+            pltpu.VMEM((n, rows + half, two), bf),
+            pltpu.VMEM((n, rows + half, two), bf),
+            pltpu.VMEM((n, 8, rows), jnp.int32),
+            pltpu.VMEM((n, half, two), bf),
+            pltpu.VMEM((n, half, two), bf),
+            pltpu.VMEM((dm, width), bf),
+            pltpu.VMEM((dm, width), bf),
+            pltpu.VMEM((width, dm), bf),
+            pltpu.VMEM(out_weight.shape, bf),
+            pltpu.VMEM((rows, local), bf),
+            pltpu.VMEM((2,) + block, bf),
+            pltpu.VMEM(block, bf),
+            pltpu.VMEM(block, f32),
+            pltpu.VMEM((n,) + block, bf),
+            pltpu.VMEM((n,) + block, bf),
+            pltpu.VMEM((levels, half // 2, dm), bf),
+            pltpu.VMEM((levels, half // 2, dm), bf),
+            pltpu.VMEM((levels,) + block, bf),
+            pltpu.VMEM((levels,) + block, bf),
+            pltpu.VMEM((levels,) + block, bf),
+            dma((n,)), dma((n,)), dma((n,)), dma((n,)), dma((n,)), dma((n,)),
+            dma((3, per)), dma((3, n)), dma((3, n // 2)), dma((3,)),
+            dma, dma, dma, dma((12, levels)), dma((12, levels)),
+        ],
+        compiler_params=pltpu.CompilerParams(has_side_effects=True, vmem_limit_bytes=60 << 20),
+    )(
+        queries, keys, values, jnp.broadcast_to(doc_ids[None], (8, rows)), score_offset,
+        gate_weight, up_weight, down_weight, resid, norm_gain[None], out_weight,
+    )
 
 
 def on_device(*args):
@@ -412,10 +584,11 @@
     dim = queries.shape[1] // score_offset.shape[0]
     fits = (
         ntp == 2
+        and n >= 4
+        and n & (n - 1) == 0
         and score_offset.shape[0] == n
         and 2 * dim == 128
         and doc_ids.shape[0] == 128
-        and n % 2 == 0
         and gate_weight.shape[1] * ntp % (n * 128) == 0
         and gate_weight.shape[0] % 128 == 0
     )

time: 312 us -> 192 us (0.62); the launches traced: 307 us -> 192 us
  waiting for transfers between devices: 177 us -> 0 us
  Pallas kernels: 86.1 us -> 189 us
  matrix products: 17.9 us -> 0 us
  between operations: 13.2 us -> 0.01 us
  local copies, waits for them, and re-layouts: 8.5 us -> 2.92 us
  other arithmetic: 4.66 us -> 0 us
    pallas_call x1, Pallas kernels: 86.1 us -> 189 us  [resharded(): pl.pallas_call(functools.partial(layer_kernel, n), out_shape=jax.ShapeDty...]
    reduce_scatter x2 -> x0, waiting for transfers between devices: 102 us -> none  [the longest x1 92.5 us: resharded(): feed = lax.psum_scatter(partial_out, 'sp', scatter_dimension=0, tiled=True)]
    all_gather x1 -> x0, waiting for transfers between devices: 74.9 us -> none  [resharded(): every = lax.all_gather(normed, 'sp', axis=0, tiled=True)]
    dot_general x3 -> x0, matrix products: 17.9 us -> none  [the longest x1 8.33 us: resharded(): jnp.dot(hidden, wd, preferred_element_type=jnp.float32).astype(jnp.bfloat16)]
    unnamed x22 -> x1, local copies, waits for them, and re-layouts: 6.92 us -> 1.67 us
    convert_element_type x2 -> x0, other arithmetic: 3.52 us -> none  [the longest x1 1.77 us: resharded(): normed = (stream * lax.rsqrt(jnp.mean(stream * stream, axis=1, keepdims=T...]
  transfers between devices with their start and end apart: 3 -> 0, of which waited for: 3 -> 0; matrix products, arithmetic and copies ran while one was open for 0% -> 0% of each run, Pallas kernels for 0% -> 0%
where the time goes in v2:
time: 192 us
  Pallas kernels  189 us (98%)
  local copies, waits for them, and re-layouts  2.92 us (2%)
    pallas_call x1, Pallas kernels, resharded(): pl.pallas_call(functools.partial(layer_kernel, n), out_shape=jax.ShapeDty...  189 us

profile of v2, /device:TPU:17, one launch (start us, length us, event | category | flops | bytes accessed | tf_op | source)
XLA Modules:
  0.0 192.2 jit_solution(4685617033838993837)
XLA Ops:
  0.0 1.2 broadcast_in_dim.4.doc_ref
  1.2 189.3 %shard_map.109 = bf16[64,2048]{1,0:T(8,128)(2,1)} custom-call(bf16[128,1024]{1,0:T(8,128)(2,1)} %q_ref.1, bf16[128,1024]{1,0:T(8,128)(2,1)} %k_ref.1, bf16[128,1024]{1,0:T(8,128)(2,1)} %v_ref.1, s32[8,128]{1,0:T(8,128)} %broadcast_in_dim.4.doc_ref, f32[16]{0:T(128)} %off_ref.1, bf16[128,3072]{1,0:T(8,128)(2,1)} %g_in.1, bf16[128,3072]{1,0:T(8,128)(2,1)} %u_in.1, ...), custom_call_target="tpu_custom_call" | custom-call | tf_op jit(solution)/shard_map/pallas_call | solution.py:544
  190.6 1.7 copy.13

commit v3 on v2

--- a/solution.py
+++ b/solution.py
@@ -164,6 +164,14 @@
     dcols = d_in.shape[1]
     back = -(-DOC_MOST // rows)
     other = 1 - c
+    barrier = pltpu.get_barrier_semaphore()
+
+    def greet(k, _):
+        pl.semaphore_signal(barrier, inc=1, device_id={"sp": lax.rem(s + k, n)}, device_id_type=MESH)
+        return 0
+
+    lax.fori_loop(1, n, greet, 0)
+    pl.semaphore_signal(barrier, inc=1, device_id={"tp": other}, device_id_type=MESH)
     pltpu.make_async_copy(o_in, ow, o_sem).start()
 
     for j in range(n // 2):
@@ -177,6 +185,8 @@
         sbuf[2 * j, rows:, :] = jnp.where(lowh, top, pltpu.roll(bot, dim, 1)).astype(jnp.bfloat16)
         sbuf[2 * j + 1, rows:, :] = jnp.where(lowh, pltpu.roll(top, dim, 1), bot).astype(jnp.bfloat16)
 
+    pl.semaphore_wait(barrier, n)
+
     def qkv_copy(t, src):
         return sends(sbuf.at[t], rbuf.at[src], qkv_s.at[t], qkv_r.at[src], {"sp": t})
 
@@ -193,7 +203,7 @@
     rbuf[pl.ds(s, 1)] = sbuf[pl.ds(s, 1)]
     docr[pl.ds(s, 1)] = doc_ref[...][None]
 
-    tc = lax.rem(s, 2)
+    tc = c
     mats = ((g_in, wg), (u_in, wu), (d_in, wd))
 
     def part_of(m, p):
@@ -211,9 +221,8 @@
     def own_copy(m, p):
         return pltpu.make_async_copy(part_of(m, p), slot_of(m, s), own_sem.at[m])
 
-    for m in range(3):
-
-        def start_weight(k, _, m=m):
+    def start_weights(m):
+        def start_weight(k, _):
             p = per * c + lax.rem(s + k, per)
             mine = (p == s) & (tc == c)
 
@@ -228,6 +237,9 @@
             return 0
 
         lax.fori_loop(0, per, start_weight, 0)
+
+    start_weights(0)
+    start_weights(1)
 
     def wait_peer(k, _):
         src = lax.rem(s + n - k, n)
@@ -292,6 +304,8 @@
 
     lax.fori_loop(0, n, block, 0)
 
+    start_weights(2)
+
     def wait_attended(k, _):
         src = lax.rem(s + n - k, n)
         att_copy(src, src).wait_recv()
@@ -383,6 +397,38 @@
     def rs_z(k):
         return link(11, k, part.at[ids(k)[0]], zr.at[k], ids(k)[0])
 
+    def forward(m, src, k):
+        return sends(slot_of(m, src), slot_of(m, src), f_s.at[m, k], w_r.at[m, src], {"tp": other})
+
+    base_c = s // per
+    def hand_on(m):
+        def pass_on(src, _):
+            mine = src == s
+
+            @pl.when(mine)
+            def _():
+                own_copy(m, s).wait()
+
+            @pl.when(jnp.logical_not(mine))
+            def _():
+                forward(m, src, src).wait_recv()
+
+            forward(m, src, src).start()
+            return 0
+
+        @pl.when(base_c == c)
+        def _():
+            lax.fori_loop(0, n, pass_on, 0)
+
+    def arrive(m):
+        def arrived(src, _):
+            forward(m, src, src).wait_recv()
+            return 0
+
+        @pl.when(base_c != c)
+        def _():
+            lax.fori_loop(0, n, arrived, 0)
+
     def spread(k):
         if k > 0:
             ag_z(k).wait_recv()
@@ -398,11 +444,20 @@
     def feed_forward(k):
         ag_hx(k).wait_recv()
         ag_hy(k).wait_recv()
+        if k == order[0]:
+            for m in range(2):
+                hand_on(m)
+            for m in range(2):
+                arrive(m)
         base = flip(s - lax.rem(s, 4), 4 * k)
         x = ag[pl.ds(base, 4)].reshape(4 * half, dm)
         gate = jnp.dot(x, wg[...], preferred_element_type=jnp.float32)
         upper = jnp.dot(x, wu[...], preferred_element_type=jnp.float32)
         hidden = (gate / (1.0 + jnp.exp(-gate)) * upper).astype(jnp.bfloat16)
+
+        if k == order[0]:
+            hand_on(2)
+            arrive(2)
 
         def columns(t, _):
             cols = pl.ds(pl.multiple_of(t * tile, tile), tile)
@@ -438,50 +493,23 @@
     spread(0)
     for k in range(1, levels):
         ag_z(k).start()
-
-    def forward(m, src, k):
-        return sends(slot_of(m, src), slot_of(m, src), f_s.at[m, k], w_r.at[m, src], {"tp": other})
-
-    base_c = s // per
-    for m in range(3):
-
-        def pass_on(k, _, m=m):
-            src = 2 * k + c
-            mine = (src == s) & (base_c == c)
-
-            @pl.when(mine)
-            def _():
-                own_copy(m, s).wait()
-
-            @pl.when(jnp.logical_not(mine))
-            def _():
-                forward(m, src, k).wait_recv()
-
-            forward(m, src, k).start()
-            return 0
-
-        lax.fori_loop(0, n // 2, pass_on, 0)
-
-    for m in range(3):
-
-        def arrived(k, _, m=m):
-            forward(m, 2 * k + other, k).wait_recv()
-            return 0
-
-        lax.fori_loop(0, n // 2, arrived, 0)
-
-    relay(0)
-    for k in range(levels + 2):
-        if k + 1 < levels:
-            spread(k + 1)
-        if k < levels:
-            feed_forward(k)
-        if 1 <= k <= levels:
-            add_relayed(k - 1)
-        if k >= 2:
-            collect(k - 2)
-        if k + 1 < levels:
-            relay(k + 1)
+    ahead = min(levels, 2)
+    for k in range(ahead):
+        if k > 0:
+            spread(k)
+        relay(k)
+    order = [*range(1, levels), 0]
+    for at in range(levels + 2):
+        if at + ahead < levels:
+            spread(at + ahead)
+        if at < levels:
+            feed_forward(order[at])
+        if 1 <= at <= levels:
+            add_relayed(order[at - 1])
+        if at >= 2:
+            collect(order[at - 2])
+        if at + ahead < levels:
+            relay(at + ahead)
     for k in range(1, levels):
         rs_z(k).wait_recv()
     out = stream[...]
@@ -507,11 +535,13 @@
     lax.fori_loop(1, n, finish_peer, 0)
     for m in range(3):
 
-        def finish_forward(k, _, m=m):
-            forward(m, 2 * k + c, k).wait_send()
+        def finish_forward(src, _, m=m):
+            forward(m, src, src).wait_send()
             return 0
 
-        lax.fori_loop(0, n // 2, finish_forward, 0)
+        @pl.when(base_c == c)
+        def _():
+            lax.fori_loop(0, n, finish_forward, 0)
 
         def finish_weight(k, _, m=m):
             p = per * c + lax.rem(s + k, per)
@@ -568,10 +598,10 @@
             pltpu.VMEM((levels,) + block, bf),
             pltpu.VMEM((levels,) + block, bf),
             dma((n,)), dma((n,)), dma((n,)), dma((n,)), dma((n,)), dma((n,)),
-            dma((3, per)), dma((3, n)), dma((3, n // 2)), dma((3,)),
+            dma((3, per)), dma((3, n)), dma((3, n)), dma((3,)),
             dma, dma, dma, dma((12, levels)), dma((12, levels)),
         ],
-        compiler_params=pltpu.CompilerParams(has_side_effects=True, vmem_limit_bytes=60 << 20),
+        compiler_params=pltpu.CompilerParams(has_side_effects=True, collective_id=0, vmem_limit_bytes=60 << 20),
     )(
         queries, keys, values, jnp.broadcast_to(doc_ids[None], (8, rows)), score_offset,
         gate_weight, up_weight, down_weight, resid, norm_gain[None], out_weight,

time: 192 us -> 171 us (0.89)
  Pallas kernels: 189 us -> 168 us
    pallas_call x1, Pallas kernels: 189 us -> 168 us  [resharded(): pl.pallas_call(functools.partial(layer_kernel, n), out_shape=jax.ShapeDty...]
where the time goes in v3:
time: 171 us
  Pallas kernels  168 us (98%)
  local copies, waits for them, and re-layouts  2.92 us (2%)
    pallas_call x1, Pallas kernels, resharded(): pl.pallas_call(functools.partial(layer_kernel, n), out_shape=jax.ShapeDty...  168 us

profile of v3, /device:TPU:17, one launch (start us, length us, event | category | flops | bytes accessed | tf_op | source)
XLA Modules:
  0.0 171.3 jit_solution(17419683142355881353)
XLA Ops:
  0.0 1.2 broadcast_in_dim.4.doc_ref
  1.2 168.4 %shard_map.109 = bf16[64,2048]{1,0:T(8,128)(2,1)} custom-call(bf16[128,1024]{1,0:T(8,128)(2,1)} %q_ref.1, bf16[128,1024]{1,0:T(8,128)(2,1)} %k_ref.1, bf16[128,1024]{1,0:T(8,128)(2,1)} %v_ref.1, s32[8,128]{1,0:T(8,128)} %broadcast_in_dim.4.doc_ref, f32[16]{0:T(128)} %off_ref.1, bf16[128,3072]{1,0:T(8,128)(2,1)} %g_in.1, bf16[128,3072]{1,0:T(8,128)(2,1)} %u_in.1, ...), custom_call_target="tpu_custom_call" | custom-call | tf_op jit(solution)/shard_map/pallas_call | solution.py:574
  169.6 1.7 copy.13

commit v4 on v3

--- a/solution.py
+++ b/solution.py
@@ -304,7 +304,6 @@
 
     lax.fori_loop(0, n, block, 0)
 
-    start_weights(2)
 
     def wait_attended(k, _):
         src = lax.rem(s + n - k, n)
@@ -493,7 +492,8 @@
     spread(0)
     for k in range(1, levels):
         ag_z(k).start()
-    ahead = min(levels, 2)
+    start_weights(2)
+    ahead = min(levels, 3)
     for k in range(ahead):
         if k > 0:
             spread(k)

time: 171 us -> 170 us (level)
  no operation moved by 1% of the time
where the time goes in v4:
time: 170 us
  Pallas kernels  167 us (98%)
  local copies, waits for them, and re-layouts  2.92 us (2%)
    pallas_call x1, Pallas kernels, resharded(): pl.pallas_call(functools.partial(layer_kernel, n), out_shape=jax.ShapeDty...  167 us

profile of v4, /device:TPU:17, one launch (start us, length us, event | category | flops | bytes accessed | tf_op | source)
XLA Modules:
  0.0 169.7 jit_solution(8402133379922143591)
XLA Ops:
  0.0 1.2 broadcast_in_dim.4.doc_ref
  1.2 166.7 %shard_map.109 = bf16[64,2048]{1,0:T(8,128)(2,1)} custom-call(bf16[128,1024]{1,0:T(8,128)(2,1)} %q_ref.1, bf16[128,1024]{1,0:T(8,128)(2,1)} %k_ref.1, bf16[128,1024]{1,0:T(8,128)(2,1)} %v_ref.1, s32[8,128]{1,0:T(8,128)} %broadcast_in_dim.4.doc_ref, f32[16]{0:T(128)} %off_ref.1, bf16[128,3072]{1,0:T(8,128)(2,1)} %g_in.1, bf16[128,3072]{1,0:T(8,128)(2,1)} %u_in.1, ...), custom_call_target="tpu_custom_call" | custom-call | tf_op jit(solution)/shard_map/pallas_call | solution.py:574
  168.0 1.7 copy.13
